TPU v7x, 512 devices: a whole 4x8x8 slice. The times are simulated.
512 devices in a mesh: sp: 64 (over z, y), tp: 8 (over x, core).
Axes of the slice: x: 4, y: 8, z: 8, core: 2. Of those that a mesh axis runs over, the one named last changes fastest.
Arguments:
- tokens: bfloat16 [16384, 2048], P(('sp', 'tp')), may hold values from -6 to 6
- gain: float32 [2048], replicated, may hold values from 0.1 to 1.9
- w_ret_q: bfloat16 [2048, 2048], P(None, 'tp'), may hold values from -0.125 to 0.125
- w_ret_k: bfloat16 [2048, 2048], P(None, 'tp'), may hold values from -0.125 to 0.125
- w_ret_v: bfloat16 [2048, 2048], P(None, 'tp'), may hold values from -0.125 to 0.125
- w_fox_q: bfloat16 [2048, 1024], P(None, 'tp'), may hold values from -0.125 to 0.125
- w_fox_k: bfloat16 [2048, 1024], P(None, 'tp'), may hold values from -0.125 to 0.125
- w_fox_v: bfloat16 [2048, 1024], P(None, 'tp'), may hold values from -0.125 to 0.125
- fox_gates: float32 [16384, 8], P('sp', 'tp'), may hold values from -16384 to 0, as said below
- w_out_ret: bfloat16 [2048, 2048], P('tp', 'sp'), may hold values from -0.109375 to 0.109375
- w_out_fox: bfloat16 [1024, 2048], P('tp', 'sp'), may hold values from -0.109375 to 0.109375
Outputs:
- mixed: bfloat16 [16384, 2048], P(('sp', 'tp'))
Inputs may be any that keep to these rules, and one draw needn't show every extreme that they name: `fox_gates`: each head's values never rise along positions.
All inputs are finite; a program needn't handle non-finite values.
Results may differ from a plain program's by a relative error of at most 0.02.
Values may be sent and summed in bfloat16 or wider, within the bound.
No kernel may reach another device: no remote copies, remote signals or barrier semaphores. Data moves between devices by JAX's collectives and lax.ppermute only.
A program may use at most 128 MiB of HBM per device.

v0:
```python
import math
import jax
import jax.numpy as jnp
from jax import lax
from jax.sharding import Mesh
from jax.sharding import PartitionSpec as P

RET_HEADS = 8
RET_DIM = 256
FOX_DIM = 128
BLOCK = 128
SP = ("sp_0", "sp_1")
SP_TP = ("sp_0", "sp_1", "tp")
eps = 1e-06


def joined_along(pieces, dim):
    dims = list(pieces.shape[1:])
    dims[dim] *= pieces.shape[0]
    return jnp.moveaxis(pieces, 0, dim).reshape(dims)


def sent_to_all(shard, axis):
    size = lax.axis_size(axis)
    return lax.all_to_all(
        jnp.broadcast_to(shard[None], (size, *shard.shape)), axis, 0, 0, tiled=True
    )


def gathered_copies(shard, axis, dim):
    return joined_along(sent_to_all(shard, axis), dim)


def filled_with(shard, identity):
    return jax.tree.map(
        lambda part, zero: jnp.zeros_like(part) + jnp.asarray(zero, part.dtype), shard, identity
    )


def entering(shard, axes, combine, identity):
    before = start = filled_with(shard, identity)
    subtotal = shard
    for axis in reversed(axes):
        size, index = (lax.axis_size(axis), lax.axis_index(axis))
        pieces = jax.tree.map(lambda part: lax.all_gather(part, axis), subtotal)
        inside, subtotal = (start, start)
        for k in range(size):
            passed = k < index
            subtotal = combine(subtotal, jax.tree.map(lambda part: part[k], pieces))
            inside = jax.tree.map(lambda new, old: jnp.where(passed, new, old), subtotal, inside)
        before = combine(inside, before)
    return before


def side_by_side(arrays, axis, dim, along):
    widths = [a.shape[along] for a in arrays]
    both = jnp.concatenate(arrays, axis=along)
    out = lax.all_gather(both, axis, axis=dim, tiled=True)
    return tuple(jnp.split(out, [sum(widths[:k]) for k in range(1, len(widths))], axis=along))


def rows_first(arrays, axis, dims):
    turned = [jnp.moveaxis(a, dim, 0) for a, dim in zip(arrays, dims)]
    widths = [t[0].size for t in turned]
    both = jnp.concatenate([t.reshape(-1, w) for t, w in zip(turned, widths)], axis=1)
    out = lax.all_gather(both, axis, axis=0, tiled=True)
    pieces = jnp.split(out, [sum(widths[:k]) for k in range(1, len(widths))], axis=1)
    return tuple(
        (
            jnp.moveaxis(b.reshape(-1, *t.shape[1:]), 0, dim)
            for b, t, dim in zip(pieces, turned, dims)
        )
    )


def in_blocks(shard, dim, size):
    before, after = (shard.shape[:dim], shard.shape[dim + 1 :])
    return jnp.moveaxis(shard.reshape(*before, size, -1, *after), dim, 0)


def sent_and_summed(shard, axis, dim):
    size = lax.axis_size(axis)
    pieces = lax.all_to_all(in_blocks(shard, dim, size), axis, 0, 0, tiled=True)
    return jnp.sum(pieces.astype(jnp.float32), axis=0)


def head_norm(values, width):
    rows_here = values.shape[0]
    grouped = values.reshape(rows_here, -1, width)
    scaled = grouped * lax.rsqrt(jnp.mean(grouped * grouped, axis=2, keepdims=True) + eps)
    return scaled.reshape(rows_here, -1).astype(jnp.bfloat16)


def rotate(values, token_positions, width):
    rows_here = values.shape[0]
    half_width = width // 2
    inverse = 10000.0 ** (-jnp.arange(half_width, dtype=jnp.float32) / half_width)
    angles = token_positions.astype(jnp.float32)[:, None] * inverse[None, :]
    cosine = jnp.cos(angles)[:, None, :]
    sine = jnp.sin(angles)[:, None, :]
    grouped = values.astype(jnp.float32).reshape(rows_here, -1, width)
    first_half = grouped[..., :half_width]
    second_half = grouped[..., half_width:]
    turned = jnp.concatenate(
        [first_half * cosine - second_half * sine, first_half * sine + second_half * cosine],
        axis=-1,
    )
    return turned.reshape(rows_here, -1)


def decay_rates(head_ids, total):
    heads_float = head_ids.astype(jnp.float32)
    middle = RET_HEADS // 2
    fast_rate = 1.0 / (32.0 + 16.0 * heads_float)
    slow_rate = jnp.exp2(-(heads_float - middle)) / total
    return jnp.where(head_ids < middle, fast_rate, slow_rate)


def decay_tables(rates):
    offsets = jnp.arange(BLOCK, dtype=jnp.float32)
    spread = offsets[:, None] - offsets[None, :]
    causal = spread >= 0
    within = jnp.where(
        causal[None], jnp.exp(-rates[:, None, None] * jnp.where(causal, spread, 0.0)[None]), 0.0
    )
    query_decay = jnp.exp(-rates[None, :] * (offsets[:, None] + 1.0))
    key_decay = jnp.exp(-rates[None, :] * (BLOCK - 1.0 - offsets[:, None]))
    block_decay = jnp.exp(-rates * BLOCK)
    return (within, query_decay, key_decay, block_decay)


def advance(carry, key_block, value_block, key_decay, block_decay):
    scaled = (key_block.astype(jnp.float32) * key_decay[:, :, None]).astype(jnp.bfloat16)
    update = jnp.einsum("shd,she->hde", scaled, value_block, preferred_element_type=jnp.float32)
    return carry * block_decay[:, None, None] + update


def retention_blocks(queries, keys, values, rates, state, heads):
    within, query_decay, key_decay, block_decay = decay_tables(rates)
    count = queries.shape[0] // BLOCK

    def shaped(array):
        return array.reshape(count, BLOCK, heads, RET_DIM)

    def step(carry, blocks):
        query_block, key_block, value_block = blocks
        scores = (
            jnp.einsum("thd,shd->hts", query_block, key_block, preferred_element_type=jnp.float32)
            * within
        )
        inner = jnp.einsum(
            "hts,she->the",
            scores.astype(jnp.bfloat16),
            value_block,
            preferred_element_type=jnp.float32,
        )
        cross = (
            jnp.einsum("thd,hde->the", query_block.astype(jnp.float32), carry)
            * query_decay[:, :, None]
        )
        return (advance(carry, key_block, value_block, key_decay, block_decay), inner + cross)

    final_state, outputs = lax.scan(step, state, (shaped(queries), shaped(keys), shaped(values)))
    return (final_state, outputs.reshape(count * BLOCK, heads * RET_DIM))


def join_states(earlier, later):
    return (earlier[0] * later[0], earlier[1] * later[0][:, None, None] + later[1])


def fox_weights(queries, keys, query_gates, key_gates, query_pos, key_pos):
    scores = jnp.einsum(
        "qhd,khd->hqk", queries, keys, preferred_element_type=jnp.float32
    ) * FOX_DIM ** (-0.5)
    scores = scores + query_gates.T[:, :, None] - key_gates.T[:, None, :]
    allowed = key_pos[None, :] <= query_pos[:, None]
    return jnp.exp(jnp.where(allowed[None], scores, -jnp.inf))


def add_block(numer, denom, weights, values):
    numer = numer + jnp.einsum(
        "hqk,khd->qhd", weights.astype(jnp.bfloat16), values, preferred_element_type=jnp.float32
    )
    denom = denom + jnp.sum(weights, axis=2).T
    return (numer, denom)


def per_device(
    tokens,
    gain,
    w_ret_q,
    w_ret_k,
    w_ret_v,
    w_fox_q,
    w_fox_k,
    w_fox_v,
    fox_gates,
    w_out_ret,
    w_out_fox,
):
    inputs = tokens.astype(jnp.float32)
    normed = (
        inputs * lax.rsqrt(jnp.mean(inputs * inputs, axis=1, keepdims=True) + eps) * gain
    ).astype(jnp.bfloat16)
    weights_in = (w_ret_q, w_ret_k, w_ret_v, w_fox_q, w_fox_k, w_fox_v)
    piece = gathered_copies(normed, "tp", 0)
    products = [jnp.dot(piece, matrix, preferred_element_type=jnp.float32) for matrix in weights_in]
    projected = jnp.concatenate(products, axis=1).astype(jnp.bfloat16)
    ret_width = w_ret_q.shape[1]
    fox_width = w_fox_q.shape[1]
    edges = [
        0,
        ret_width,
        2 * ret_width,
        3 * ret_width,
        3 * ret_width + fox_width,
        3 * ret_width + 2 * fox_width,
        3 * ret_width + 3 * fox_width,
    ]
    pieces_out = [projected[:, edges[column] : edges[column + 1]] for column in range(6)]
    ret_query, ret_key, ret_value, fox_query, fox_key, fox_value = pieces_out
    length = projected.shape[0]
    sp_count = lax.axis_size(SP)
    total = length * sp_count
    offset = lax.axis_index(SP) * length
    token_positions = offset + jnp.arange(length, dtype=jnp.int32)
    ret_heads = ret_width // RET_DIM
    fox_heads = fox_width // FOX_DIM
    head_ids = lax.axis_index("tp") * ret_heads + jnp.arange(ret_heads, dtype=jnp.int32)
    rates = decay_rates(head_ids, float(total))
    query_rot = rotate(ret_query, token_positions, RET_DIM).astype(jnp.bfloat16)
    key_rot = (rotate(ret_key, token_positions, RET_DIM) * RET_DIM ** (-0.5)).astype(jnp.bfloat16)
    span_decay = jnp.exp(-rates * length)
    empty_state = jnp.zeros((ret_heads, RET_DIM, RET_DIM), jnp.float32)
    identity = (jnp.ones_like(span_decay), empty_state)
    final_state, local_part = retention_blocks(
        query_rot, key_rot, ret_value, rates, empty_state, ret_heads
    )
    carried = entering((span_decay, final_state), SP, join_states, identity)[1]
    query_up = query_rot.astype(jnp.float32).reshape(length, ret_heads, RET_DIM)
    steps_in = jnp.arange(length, dtype=jnp.float32)
    reach = jnp.exp(-rates[None, :] * (steps_in[:, None] + 1.0))
    carried_part = jnp.einsum("thd,hde->the", query_up, carried) * reach[:, :, None]
    ret_raw = local_part + carried_part.reshape(length, ret_width)
    ret_mixed = head_norm(ret_raw, RET_DIM)
    gates_all = gathered_copies(fox_gates, SP, 0)
    query3 = fox_query.reshape(length, fox_heads, FOX_DIM)
    zero_numer = jnp.zeros((length, fox_heads, FOX_DIM), jnp.float32)
    zero_denom = jnp.zeros((length, fox_heads), jnp.float32)
    last_query = offset + length - 1
    keys, values = side_by_side((fox_key, fox_value), SP, 0, 1)
    rows_here = keys.shape[0]
    width = math.gcd(rows_here, 512)

    def one_block(state, index):
        begin = index * width

        def compute(accum):
            key_block = lax.dynamic_slice_in_dim(keys, begin, width, 0).reshape(
                width, fox_heads, FOX_DIM
            )
            value_block = lax.dynamic_slice_in_dim(values, begin, width, 0).reshape(
                width, fox_heads, FOX_DIM
            )
            key_gates = lax.dynamic_slice_in_dim(gates_all, begin, width, 0)
            key_pos = begin + jnp.arange(width, dtype=jnp.int32)
            weights = fox_weights(query3, key_block, fox_gates, key_gates, token_positions, key_pos)
            return add_block(accum[0], accum[1], weights, value_block)

        def skip(accum):
            return accum

        return (lax.cond(begin <= last_query, compute, skip, state), None)

    result, _ = lax.scan(
        one_block, (zero_numer, zero_denom), jnp.arange(rows_here // width, dtype=jnp.int32)
    )
    numer, denom = result
    fox_raw = (numer / denom[:, :, None]).reshape(length, fox_width)
    fox_mixed = head_norm(fox_raw, FOX_DIM)
    out_ret, out_fox = rows_first((w_out_ret, w_out_fox), SP, (1, 1))
    summed = sent_and_summed(
        (
            jnp.dot(ret_mixed, out_ret, preferred_element_type=jnp.float32)
            + jnp.dot(fox_mixed, out_fox, preferred_element_type=jnp.float32)
        ).astype(jnp.bfloat16),
        "tp",
        0,
    )
    return summed.astype(jnp.bfloat16)


def solution(mesh):
    split = Mesh(mesh.devices.reshape(8, 8, mesh.shape["tp"]), ("sp_0", "sp_1", "tp"))
    return jax.shard_map(
        per_device,
        mesh=split,
        in_specs=(
            P(SP_TP, None),
            P(),
            P(None, "tp"),
            P(None, "tp"),
            P(None, "tp"),
            P(None, "tp"),
            P(None, "tp"),
            P(None, "tp"),
            P(SP, "tp"),
            P("tp", SP),
            P("tp", SP),
        ),
        out_specs=P(SP_TP, None),
        check_vma=False,
    )
```

profile of v0, /device:TPU:496, one launch (start us, length us, event | category | flops | bytes accessed | tf_op | source)
XLA Modules:
  0.0 491.8 jit_solution(2575343854345460355)
XLA Ops:
  9.8 4.3 all-to-all-start
  14.3 15.7 %all-to-all-done = bf16[8,32,2048]{2,1,0:T(8,128)(2,1)S(1)} async-done(((bf16[8,32,2048]{2,1,0:T(8,128)(2,1)}), bf16[8,32,2048]{2,1,0:T(8,128)(2,1)S(1)}, u32[]{:S(2)}, u32[]{:S(2)}) %all-to-all-start) | async-done | bytes 1048608 | tf_op jit(solution)/shard_map/all_to_all | solution.py:25
  30.5 1.8 fusion.70
  33.7 7.6 %while.29 = (s32[]{:T(128)}, f32[1,256,256]{2,1,0:T(8,128)S(1)}, f32[2,128,1,256]{1,0,3,2:T(2,128)S(1)}, f32[1]{0:T(128)}, bf16[2,128,1,256]{3,1,2,0:T(8,128)(2,...) while((s32[]{:T(128)}, f32[1,256,256]{2,1,0:T(8,128)S(1)}, ...), condition=%wide.region_2.3_spmd.clone.clone.clone, body=%wide.region_1.2_spmd.clone.clone.clone.sunk | while | flops 50872832 | bytes 1840267 | solution.py:163
  34.3 2.9 dynamic_update_slice.8
  38.1 2.9 dynamic_update_slice.8
  42.1 1.3 dynamic-slice
  44.1 14.3 %all-reduce = f32[8]{0:T(128)S(1)} all-reduce(f32[8]{0:T(128)S(1)} %dynamic-update-slice), channel_id=2, replica_groups=mesh['sp_0'=8,'sp_1'=8,'tp'=8] {'sp_1'}, use_global_device_ids=true, to_apply=%add | all-reduce | flops 8 | bytes 64
  59.0 1.3 slice_multiply_fusion
  60.9 20.0 %all-gather.14.cloned.1.call-done = f32[8,256,256]{2,1,0:T(8,128)} async-done(((f32[1,256,256]{2,1,0:T(8,128)}), f32[8,256,256]{2,1,0:T(8,128)}) %all-gather.14.cloned.1.call-update) | async-done | bytes 2097168 | tf_op jit(solution)/shard_map/all_gather | solution.py:45
  80.9 6.7 %bitcast_add_fusion.4 = f32[1,1,256,256]{3,2,1,0:T(8,128)} fusion(f32[8,256,256]{2,1,0:T(8,128)} %all-gather.14.cloned.1.call-done, f32[]{:T(128)} %bitcast.32, f32[]{:T(128)} %bitcast.30, f32[]{:T(128)} %bitcast.28, f32[]{:T(128)} %bitcast.26, f32[]{:T(128)} %bitcast.24, f32[]{:T(128)} %bitcast.23, f32[]{:T(128)} %bitcast.22, f32[]{:T(128)} %bitcast.21), kind=kLoop, calls=%fused_computation.120 | loop fusion | flops 983040 | bytes 2359328 | tf_op jit(solution)/shard_map/add | solution.py:168
  87.7 1.3 pad_maximum_fusion.2
  90.7 1.3 dynamic-slice.1
  92.0 1.3 dynamic-update-slice.1
  93.4 1.3 broadcast_in_dim.33
  94.7 11.7 %all-to-all-start.1 = ((f32[64,256,1]{1,2,0:T(1,128)}), f32[64,256,1]{1,2,0:T(1,128)S(1)}, u32[]{:S(2)}, u32[]{:S(2)}) async-start(f32[64,256,1]{1,2,0:T(1,128)} %broadcast_in_dim.33), calls=%async_computation.1 | async-start | bytes 131072 | tf_op jit(solution)/shard_map/all_to_all | solution.py:25
  106.4 15.3 %all-reduce.1 = f32[8]{0:T(128)S(1)} all-reduce(f32[8]{0:T(128)S(1)} %dynamic-update-slice.1), channel_id=3, replica_groups=mesh['sp_0'=8,'sp_1'=8,'tp'=8] {'sp_0'}, use_global_device_ids=true, to_apply=%add.1 | all-reduce | flops 8 | bytes 64
  129.4 1.7 all-gather.8.cloned.1.call-done
  131.2 11.3 %multiply_reduce_fusion = (f32[256]{0:T(256)S(1)}, f32[256,1,256]{0,2,1:T(8,128)S(1)}) fusion(f32[256,1,256]{0,2,1:T(8,128)S(1)} %reshape.652, f32[256]{0:T(256)S(1)} %multiply_exponential_fusion, bf16[256,128]{0,1:T(8,128)(2,1)S(1)} %bitcast.300, bf16[256,128]{0,1:T(8,128)(2,1)S(1)} %bitcast.299, f32[8,1,256,256]{3,2,1,0:T(8,128)} %all-gather.8.cloned.1.call-done, ...), kind=kOutput, calls=%fused_computation.139 | convolution fusion | flops 37224192 | bytes 4851796 | tf_op jit(solution)/shard_map/thd,hde->the/dot_general | solution.py:243
  142.5 71.0 %all-gather.10.cloned.1.call-done = bf16[2048,384]{1,0:T(8,128)(2,1)} async-done(((bf16[32,384]{1,0:T(8,128)(2,1)}), bf16[2048,384]{1,0:T(8,128)(2,1)}) %all-gather.10.cloned.1.call-update) | async-done | bytes 1572880 | tf_op jit(solution)/shard_map/all_gather | solution.py:66
  213.5 3.1 fusion.72
  216.6 105.2 %all-gather.12.cloned.1.call-done = bf16[16384,256]{0,1:T(8,128)(2,1)} async-done(((bf16[256,256]{0,1:T(8,128)(2,1)}), bf16[16384,256]{0,1:T(8,128)(2,1)}) %all-gather.12.cloned.1.call-update) | async-done | bytes 8388624 | tf_op jit(solution)/shard_map/all_gather | solution.py:58
  321.8 5.8 %fusion.177 = (bf16[16384,128]{0,1:T(8,128)(2,1)}, bf16[16384,128]{0,1:T(8,128)(2,1)}) fusion(bf16[16384,256]{0,1:T(8,128)(2,1)} %all-gather.12.cloned.1.call-done), kind=kLoop, calls=%fused_computation.228 | loop fusion | bytes 16777216 | tf_op jit(solution)/shard_map/split | solution.py:59
  327.6 6.4 %copy.33 = bf16[16384,128]{1,0:T(8,128)(2,1)} copy(bf16[16384,128]{0,1:T(8,128)(2,1)} %get-tuple-element.367) | data formatting | bytes 8388608
  334.0 6.4 %copy.32 = bf16[16384,128]{1,0:T(8,128)(2,1)} copy(bf16[16384,128]{0,1:T(8,128)(2,1)} %get-tuple-element.368) | data formatting | bytes 8388608
  340.4 121.7 %while.28 = (s32[]{:T(128)}, f32[256,1,128]{0,2,1:T(8,128)S(1)}, f32[256,1]{0,1:T(1,128)S(1)}, s32[32]{0:T(128)S(1)}, s32[]{:T(128)}, /*index=5*/bf16[16384,128]...) while((s32[]{:T(128)}, f32[256,1,128]{0,2,1:T(8,128)S(1)}, ...), condition=%wide.region_8.9_spmd.clone, body=%wide.region_4.8_spmd.clone.sunk | while | flops 68059904 | bytes 1133913 | solution.py:275
  341.7 2.5 conditional.3
  345.5 2.5 conditional.3
  349.3 2.5 conditional.3
  353.1 2.5 conditional.3
  353.2 1.2 fusion.176
  356.9 2.5 conditional.3
  357.0 1.2 fusion.176
  360.7 2.5 conditional.3
  364.5 2.5 conditional.3
  368.3 2.5 conditional.3
  368.5 1.2 fusion.176
  372.1 2.5 conditional.3
  372.3 1.2 fusion.176
  375.9 2.5 conditional.3
  379.7 2.5 conditional.3
  383.5 2.5 conditional.3
  387.4 2.5 conditional.3
  391.2 2.5 conditional.3
  395.0 2.5 conditional.3
  398.8 2.5 conditional.3
  402.6 2.5 conditional.3
  406.4 2.5 conditional.3
  410.2 2.5 conditional.3
  414.0 2.5 conditional.3
  417.8 2.5 conditional.3
  421.6 2.5 conditional.3
  425.4 2.5 conditional.3
  429.2 2.5 conditional.3
  433.0 2.5 conditional.3
  436.8 2.5 conditional.3
  440.6 2.5 conditional.3
  444.4 2.5 conditional.3
  448.2 2.5 conditional.3
  452.0 2.5 conditional.3
  455.8 2.5 conditional.3
  459.6 2.5 conditional.3
  462.2 2.2 fusion.63
  464.5 20.0 %all_to_all.15 = bf16[8,32,2048]{2,1,0:T(8,128)(2,1)S(1)} all-to-all(bf16[8,32,2048]{2,1,0:T(8,128)(2,1)S(1)} %bitcast.298), channel_id=1, replica_groups=mesh['sp_0'=8,'sp_1'=8,'tp'=8] {'tp'}, dimensions={0} | all-to-all | bytes 2097152 | tf_op jit(solution)/shard_map/all_to_all | solution.py:83
  (320 shorter events, 107.1 us)
Async XLA Ops:
  6.5 23.5 %copy-start = (bf16[2048,256]{1,0:T(8,128)(2,1)S(1)}, bf16[2048,256]{1,0:T(8,128)(2,1)}, u32[]{:S(2)}) copy-start(bf16[2048,256]{1,0:T(8,128)(2,1)} %param.21) | copy-start | bytes 3145732
  9.8 20.2 %all-to-all-start = ((bf16[8,32,2048]{2,1,0:T(8,128)(2,1)}), bf16[8,32,2048]{2,1,0:T(8,128)(2,1)S(1)}, u32[]{:S(2)}, u32[]{:S(2)}) async-start(bf16[8,32,2048]{2,1,0:T(8,128)(2,1)} %broadcast_in_dim.28), calls=%async_computation | async-start | bytes 2097152 | tf_op jit(solution)/shard_map/all_to_all | solution.py:25
  14.1 66.8 %all-gather.14.cloned.1.call-start = ((), (), s32[]{:S(2)}) async-start(), calls=%async_computation.6 | async-start | bytes 2359296 | tf_op jit(solution)/shard_map/all_gather | solution.py:45
  30.0 2.2 copy-start.2
  41.3 0.7 copy-start.1
  41.3 39.6 %copy-start.6 = (f32[2,128,1,256]{1,0,3,2:T(2,128)}, f32[2,128,1,256]{1,0,3,2:T(2,128)S(1)}, u32[]{:S(2)}) copy-start(f32[2,128,1,256]{1,0,3,2:T(2,128)S(1)} %get-tuple-element.149) | copy-start | bytes 786436
  41.3 46.4 %copy-start.7 = (bf16[256,32]{0,1:T(8,128)(2,1)S(1)}, bf16[256,32]{0,1:T(8,128)(2,1)}, u32[]{:S(2)}) copy-start(bf16[256,32]{0,1:T(8,128)(2,1)} %param.26) | copy-start | bytes 49156
  41.3 47.8 %copy-start.3 = (bf16[2048,128]{1,0:T(8,128)(2,1)S(1)}, bf16[2048,128]{1,0:T(8,128)(2,1)}, u32[]{:S(2)}) copy-start(bf16[2048,128]{1,0:T(8,128)(2,1)} %param.24) | copy-start | bytes 1572868
  42.0 89.2 %all-gather.8.cloned.1.call-start = ((), (), s32[]{:S(2)}) async-start(), calls=%async_computation.3 | async-start | bytes 2359296 | tf_op jit(solution)/shard_map/all_gather | solution.py:45
  80.9 8.6 %copy-start.4 = (bf16[2048,128]{1,0:T(8,128)(2,1)S(1)}, bf16[2048,128]{1,0:T(8,128)(2,1)}, u32[]{:S(2)}) copy-start(bf16[2048,128]{1,0:T(8,128)(2,1)} %param.23) | copy-start | bytes 1572868
  87.6 125.9 %all-gather.10.cloned.1.call-start = ((), (), s32[]{:S(2)}) async-start(), calls=%async_computation.4 | async-start | bytes 1597440 | tf_op jit(solution)/shard_map/all_gather | solution.py:66
  89.0 232.8 %all-gather.12.cloned.1.call-start = ((), (), s32[]{:S(2)}) async-start(), calls=%async_computation.5 | async-start | bytes 8519680 | tf_op jit(solution)/shard_map/all_gather | solution.py:58
  89.6 39.5 %copy-start.5 = (bf16[2048,128]{1,0:T(8,128)(2,1)S(1)}, bf16[2048,128]{1,0:T(8,128)(2,1)}, u32[]{:S(2)}) copy-start(bf16[2048,128]{1,0:T(8,128)(2,1)} %param.22) | copy-start | bytes 1572868
  94.7 245.7 %all-to-all-start.1 = ((f32[64,256,1]{1,2,0:T(1,128)}), f32[64,256,1]{1,2,0:T(1,128)S(1)}, u32[]{:S(2)}, u32[]{:S(2)}) async-start(f32[64,256,1]{1,2,0:T(1,128)} %broadcast_in_dim.33), calls=%async_computation.1 | async-start | bytes 131072 | tf_op jit(solution)/shard_map/all_to_all | solution.py:25
  334.0 6.5 %copy-start.8 = (f32[256,1]{0,1:T(1,128)S(1)}, f32[256,1]{0,1:T(1,128)}, u32[]{:S(2)}) copy-start(f32[256,1]{0,1:T(1,128)} %param.25) | copy-start | bytes 3076
Sparse Core Ops, SparseCore 0:
  42.1 38.7 all-gather.13
  87.7 43.3 all-gather.7
  134.2 79.2 all-gather.9
  216.3 105.3 all-gather.11
where the time goes:
time: 494 us; the launch traced here: 492 us
  waiting for transfers between devices  214 us (43%)
  matrix products  98.6 us (20%)
  local copies, waits for them, and re-layouts  55.7 us (11%)
  blocking collectives  49.6 us (10%)
  loops' own time  23.7 us (5%)
  between operations  19.7 us (4%)
  starting transfers between devices  16.1 us (3%)
  other arithmetic  14.8 us (3%)
    all_gather x1, waiting for transfers between devices, side_by_side(): out = lax.all_gather(both, axis, axis=dim, tiled=True)  105 us
    all_gather x1, waiting for transfers between devices, rows_first(): out = lax.all_gather(both, axis, axis=0, tiled=True)  71 us
    dot_general x32, matrix products, fox_weights(): jnp.einsum('qhd,khd->hqk', queries, keys, preferred_element_type=jnp.floa...  39.5 us
    dot_general x32, matrix products, add_block(): jnp.einsum('hqk,khd->qhd', weights.astype(jnp.bfloat16), values, preferre...  36.7 us
    unnamed x2, blocking collectives  29.6 us
    another operation x1, loops' own time, per_device(): lax.scan(one_block, (zero_numer, zero_denom), jnp.arange(rows_here // wid...  22.1 us
    all_gather x2, waiting for transfers between devices, entering(): pieces = jax.tree.map(lambda part: lax.all_gather(part, axis), subtotal)  21.7 us
    all_to_all x1, blocking collectives, sent_and_summed(): pieces = lax.all_to_all(in_blocks(shard, dim, size), axis, 0, 0, tiled=True)  20 us
  transfers between devices with their start and end apart: 6, of which 5 were waited for; matrix products, arithmetic and copies ran while one was open for 9% of the time, Pallas kernels for 0%

commit v1 on v0

--- a/solution.py
+++ b/solution.py
@@ -63,7 +63,9 @@
     turned = [jnp.moveaxis(a, dim, 0) for a, dim in zip(arrays, dims)]
     widths = [t[0].size for t in turned]
     both = jnp.concatenate([t.reshape(-1, w) for t, w in zip(turned, widths)], axis=1)
-    out = lax.all_gather(both, axis, axis=0, tiled=True)
+    out = jnp.concatenate(
+        lax.all_to_all(jnp.stack([both] * lax.axis_size(axis)), axis, 0, 0), axis=0
+    )
     pieces = jnp.split(out, [sum(widths[:k]) for k in range(1, len(widths))], axis=1)
     return tuple(
         (

time: 494 us -> 441 us (0.89)
  waiting for transfers between devices: 214 us -> 125 us
  blocking collectives: 49.6 us -> 73.2 us
  starting transfers between devices: 16.1 us -> 27.6 us
    all_gather x1 -> x0, waiting for transfers between devices: 71 us -> none  [rows_first(): out = lax.all_gather(both, axis, axis=0, tiled=True)]
    all_gather x1, waiting for transfers between devices: 105 us -> 80.8 us  [side_by_side(): out = lax.all_gather(both, axis, axis=dim, tiled=True)]
    unnamed x2, blocking collectives: 29.6 us -> 53.2 us
    all_to_all x0 -> x1, starting transfers between devices: none -> 12 us  [rows_first(): lax.all_to_all(jnp.stack([both] * lax.axis_size(axis)), axis, 0, 0)]
    all_gather x2, waiting for transfers between devices: 21.7 us -> 28.8 us  [entering(): pieces = jax.tree.map(lambda part: lax.all_gather(part, axis), subtotal)]
    unnamed x28 -> x32, local copies, waits for them, and re-layouts: 18.4 us -> 18.5 us
  transfers between devices with their start and end apart: 6 -> 6, of which waited for: 5 -> 4; matrix products, arithmetic and copies ran while one was open for 9% -> 10% of each run, Pallas kernels for 0% -> 0%
where the time goes in v1:
time: 441 us; the launch traced here: 438 us
  waiting for transfers between devices  125 us (28%)
  matrix products  99 us (22%)
  blocking collectives  73.2 us (17%)
  local copies, waits for them, and re-layouts  55.4 us (13%)
  starting transfers between devices  27.6 us (6%)
  loops' own time  23.7 us (5%)
  between operations  19.9 us (5%)
  other arithmetic  13.8 us (3%)
    all_gather x1, waiting for transfers between devices, side_by_side(): out = lax.all_gather(both, axis, axis=dim, tiled=True)  80.8 us
    unnamed x2, blocking collectives  53.2 us
    dot_general x32, matrix products, fox_weights(): jnp.einsum('qhd,khd->hqk', queries, keys, preferred_element_type=jnp.floa...  39.5 us
    dot_general x32, matrix products, add_block(): jnp.einsum('hqk,khd->qhd', weights.astype(jnp.bfloat16), values, preferre...  36.7 us
    all_gather x2, waiting for transfers between devices, entering(): pieces = jax.tree.map(lambda part: lax.all_gather(part, axis), subtotal)  28.8 us
    another operation x1, loops' own time, per_device(): lax.scan(one_block, (zero_numer, zero_denom), jnp.arange(rows_here // wid...  22.1 us
    all_to_all x1, blocking collectives, sent_and_summed(): pieces = lax.all_to_all(in_blocks(shard, dim, size), axis, 0, 0, tiled=True)  20 us
    dynamic_slice x32, local copies, waits for them, and re-layouts, per_device(): lax.scan(one_block, (zero_numer, zero_denom), jnp.arange(rows_here // wid...  18.8 us
  transfers between devices with their start and end apart: 6, of which 4 were waited for; matrix products, arithmetic and copies ran while one was open for 10% of the time, Pallas kernels for 0%

profile of v1, /device:TPU:496, one launch (start us, length us, event | category | flops | bytes accessed | tf_op | source)
XLA Modules:
  0.0 438.0 jit_solution(3140744757682495692)
XLA Ops:
  9.8 4.3 all-to-all-start
  14.3 15.7 %all-to-all-done = bf16[8,32,2048]{2,1,0:T(8,128)(2,1)S(1)} async-done(((bf16[8,32,2048]{2,1,0:T(8,128)(2,1)}), bf16[8,32,2048]{2,1,0:T(8,128)(2,1)S(1)}, u32[]{:S(2)}, u32[]{:S(2)}) %all-to-all-start) | async-done | bytes 1048608 | tf_op jit(solution)/shard_map/all_to_all | solution.py:25
  30.5 1.7 fusion.70
  33.6 7.6 %while.29 = (s32[]{:T(128)}, f32[1,256,256]{2,1,0:T(8,128)S(1)}, f32[2,128,1,256]{1,0,3,2:T(2,128)S(1)}, f32[1]{0:T(128)}, bf16[2,128,1,256]{3,1,2,0:T(8,128)(2,...) while((s32[]{:T(128)}, f32[1,256,256]{2,1,0:T(8,128)S(1)}, ...), condition=%wide.region_2.3_spmd.clone.clone.clone, body=%wide.region_1.2_spmd.clone.clone.clone.sunk | while | flops 50872832 | bytes 1840267 | solution.py:165
  34.3 2.9 dynamic_update_slice.8
  38.1 2.9 dynamic_update_slice.8
  42.1 1.3 dynamic-slice
  44.1 14.3 %all-reduce = f32[8]{0:T(128)S(1)} all-reduce(f32[8]{0:T(128)S(1)} %dynamic-update-slice), channel_id=2, replica_groups=mesh['sp_0'=8,'sp_1'=8,'tp'=8] {'sp_1'}, use_global_device_ids=true, to_apply=%add | all-reduce | flops 8 | bytes 64
  59.1 1.3 slice_multiply_fusion
  61.0 20.0 %all-gather.11.cloned.1.call-done = f32[8,256,256]{2,1,0:T(8,128)} async-done(((f32[1,256,256]{2,1,0:T(8,128)}), f32[8,256,256]{2,1,0:T(8,128)}) %all-gather.11.cloned.1.call-update) | async-done | bytes 2097168 | tf_op jit(solution)/shard_map/all_gather | solution.py:45
  81.0 6.8 %bitcast_add_fusion.4 = f32[1,1,256,256]{3,2,1,0:T(8,128)} fusion(f32[8,256,256]{2,1,0:T(8,128)} %all-gather.11.cloned.1.call-done, f32[]{:T(128)} %bitcast.32, f32[]{:T(128)} %bitcast.30, f32[]{:T(128)} %bitcast.28, f32[]{:T(128)} %bitcast.26, f32[]{:T(128)} %bitcast.24, f32[]{:T(128)} %bitcast.23, f32[]{:T(128)} %bitcast.22, f32[]{:T(128)} %bitcast.21), kind=kLoop, calls=%fused_computation.120 | loop fusion | flops 983040 | bytes 2359328 | tf_op jit(solution)/shard_map/add | solution.py:170
  89.6 1.3 stack.2
  91.0 12.0 %all-to-all-start.1 = ((bf16[64,32,384]{2,1,0:T(8,128)(2,1)}), bf16[64,32,384]{2,1,0:T(8,128)(2,1)}, u32[]{:S(2)}, u32[]{:S(2)}) async-start(bf16[64,32,384]{2,1,0:T(8,128)(2,1)} %stack.2), calls=%async_computation.1 | async-start | bytes 3145728 | tf_op jit(solution)/shard_map/all_to_all | solution.py:67
  103.0 1.3 dynamic-slice.1
  104.3 1.4 dynamic-update-slice.1
  105.7 38.9 %all-reduce.1 = f32[8]{0:T(128)S(1)} all-reduce(f32[8]{0:T(128)S(1)} %dynamic-update-slice.1), channel_id=3, replica_groups=mesh['sp_0'=8,'sp_1'=8,'tp'=8] {'sp_0'}, use_global_device_ids=true, to_apply=%add.1 | all-reduce | flops 8 | bytes 64
  151.6 8.8 %all-gather.7.cloned.1.call-done = f32[8,1,256,256]{3,2,1,0:T(8,128)} async-done(((f32[1,1,256,256]{3,2,1,0:T(8,128)}), f32[8,1,256,256]{3,2,1,0:T(8,128)}) %all-gather.7.cloned.1.call-update) | async-done | bytes 2097168 | tf_op jit(solution)/shard_map/all_gather | solution.py:45
  160.5 11.7 %multiply_reduce_fusion = (f32[256]{0:T(256)S(1)}, f32[256,1,256]{0,2,1:T(8,128)S(1)}) fusion(f32[256,1,256]{0,2,1:T(8,128)S(1)} %reshape.657, f32[256]{0:T(256)S(1)} %multiply_exponential_fusion, bf16[256,128]{0,1:T(8,128)(2,1)S(1)} %bitcast.301, bf16[256,128]{0,1:T(8,128)(2,1)S(1)} %bitcast.300, f32[8,1,256,256]{3,2,1,0:T(8,128)} %all-gather.7.cloned.1.call-done, ...), kind=kOutput, calls=%fused_computation.139 | convolution fusion | flops 37224192 | bytes 4851796 | tf_op jit(solution)/shard_map/thd,hde->the/dot_general | solution.py:245
  172.9 11.2 %all-to-all-start.2 = ((f32[64,256,1]{1,2,0:T(1,128)}), f32[64,256,1]{1,2,0:T(1,128)S(1)}, u32[]{:S(2)}, u32[]{:S(2)}) async-start(f32[64,256,1]{1,2,0:T(1,128)} %broadcast_in_dim.33), calls=%async_computation.2 | async-start | bytes 131072 | tf_op jit(solution)/shard_map/all_to_all | solution.py:25
  184.1 3.1 fusion.72
  187.2 80.8 %all-gather.9.cloned.1.call-done = bf16[16384,256]{0,1:T(8,128)(2,1)} async-done(((bf16[256,256]{0,1:T(8,128)(2,1)}), bf16[16384,256]{0,1:T(8,128)(2,1)}) %all-gather.9.cloned.1.call-update) | async-done | bytes 8388624 | tf_op jit(solution)/shard_map/all_gather | solution.py:58
  268.0 5.8 %fusion.177 = (bf16[16384,128]{0,1:T(8,128)(2,1)}, bf16[16384,128]{0,1:T(8,128)(2,1)}) fusion(bf16[16384,256]{0,1:T(8,128)(2,1)} %all-gather.9.cloned.1.call-done), kind=kLoop, calls=%fused_computation.228 | loop fusion | bytes 16777216 | tf_op jit(solution)/shard_map/split | solution.py:59
  273.8 6.4 %copy.33 = bf16[16384,128]{1,0:T(8,128)(2,1)} copy(bf16[16384,128]{0,1:T(8,128)(2,1)} %get-tuple-element.367) | data formatting | bytes 8388608
  280.2 6.4 %copy.32 = bf16[16384,128]{1,0:T(8,128)(2,1)} copy(bf16[16384,128]{0,1:T(8,128)(2,1)} %get-tuple-element.368) | data formatting | bytes 8388608
  286.6 121.7 %while.28 = (s32[]{:T(128)}, f32[256,1,128]{0,2,1:T(8,128)S(1)}, f32[256,1]{0,1:T(1,128)S(1)}, s32[32]{0:T(128)S(1)}, s32[]{:T(128)}, /*index=5*/bf16[16384,128]...) while((s32[]{:T(128)}, f32[256,1,128]{0,2,1:T(8,128)S(1)}, ...), condition=%wide.region_8.9_spmd.clone, body=%wide.region_4.8_spmd.clone.sunk | while | flops 68059904 | bytes 1133913 | solution.py:277
  287.9 2.5 conditional.3
  291.7 2.5 conditional.3
  295.5 2.5 conditional.3
  295.6 1.2 fusion.176
  299.3 2.5 conditional.3
  303.1 2.5 conditional.3
  306.9 2.5 conditional.3
  310.7 2.5 conditional.3
  310.8 1.2 fusion.176
  314.5 2.5 conditional.3
  314.6 1.2 fusion.176
  318.3 2.5 conditional.3
  322.1 2.5 conditional.3
  325.9 2.5 conditional.3
  326.1 1.2 fusion.176
  329.7 2.5 conditional.3
  329.9 1.2 fusion.176
  333.5 2.5 conditional.3
  337.3 2.5 conditional.3
  341.1 2.5 conditional.3
  345.0 2.5 conditional.3
  348.8 2.5 conditional.3
  352.6 2.5 conditional.3
  356.4 2.5 conditional.3
  360.2 2.5 conditional.3
  364.0 2.5 conditional.3
  367.8 2.5 conditional.3
  371.6 2.5 conditional.3
  375.4 2.5 conditional.3
  379.2 2.5 conditional.3
  383.0 2.5 conditional.3
  386.8 2.5 conditional.3
  390.6 2.5 conditional.3
  394.4 2.5 conditional.3
  398.2 2.5 conditional.3
  402.0 2.5 conditional.3
  405.8 2.5 conditional.3
  408.4 2.2 fusion.63
  410.7 20.0 %all_to_all.20 = bf16[8,32,2048]{2,1,0:T(8,128)(2,1)S(1)} all-to-all(bf16[8,32,2048]{2,1,0:T(8,128)(2,1)S(1)} %bitcast.299), channel_id=1, replica_groups=mesh['sp_0'=8,'sp_1'=8,'tp'=8] {'tp'}, dimensions={0} | all-to-all | bytes 2097152 | tf_op jit(solution)/shard_map/all_to_all | solution.py:85
  (324 shorter events, 105.6 us)
Async XLA Ops:
  6.5 23.5 %copy-start = (bf16[2048,256]{1,0:T(8,128)(2,1)S(1)}, bf16[2048,256]{1,0:T(8,128)(2,1)}, u32[]{:S(2)}) copy-start(bf16[2048,256]{1,0:T(8,128)(2,1)} %param.21) | copy-start | bytes 3145732
  9.8 20.2 %all-to-all-start = ((bf16[8,32,2048]{2,1,0:T(8,128)(2,1)}), bf16[8,32,2048]{2,1,0:T(8,128)(2,1)S(1)}, u32[]{:S(2)}, u32[]{:S(2)}) async-start(bf16[8,32,2048]{2,1,0:T(8,128)(2,1)} %broadcast_in_dim.28), calls=%async_computation | async-start | bytes 2097152 | tf_op jit(solution)/shard_map/all_to_all | solution.py:25
  14.1 66.9 %all-gather.11.cloned.1.call-start = ((), (), s32[]{:S(2)}) async-start(), calls=%async_computation.6 | async-start | bytes 2359296 | tf_op jit(solution)/shard_map/all_gather | solution.py:45
  30.0 2.2 copy-start.2
  41.2 0.7 copy-start.1
  41.3 39.7 %copy-start.6 = (f32[2,128,1,256]{1,0,3,2:T(2,128)}, f32[2,128,1,256]{1,0,3,2:T(2,128)S(1)}, u32[]{:S(2)}) copy-start(f32[2,128,1,256]{1,0,3,2:T(2,128)S(1)} %get-tuple-element.149) | copy-start | bytes 786436
  41.3 46.6 %copy-start.3 = (bf16[2048,128]{1,0:T(8,128)(2,1)S(1)}, bf16[2048,128]{1,0:T(8,128)(2,1)}, u32[]{:S(2)}) copy-start(bf16[2048,128]{1,0:T(8,128)(2,1)} %param.24) | copy-start | bytes 1572868
  42.0 118.5 %all-gather.7.cloned.1.call-start = ((), (), s32[]{:S(2)}) async-start(), calls=%async_computation.4 | async-start | bytes 2359296 | tf_op jit(solution)/shard_map/all_gather | solution.py:45
  81.0 7.4 %copy-start.4 = (bf16[2048,128]{1,0:T(8,128)(2,1)S(1)}, bf16[2048,128]{1,0:T(8,128)(2,1)}, u32[]{:S(2)}) copy-start(bf16[2048,128]{1,0:T(8,128)(2,1)} %param.23) | copy-start | bytes 1572868
  87.8 1.8 copy-start.8
  87.8 1.8 copy-start.9
  87.9 180.1 %all-gather.9.cloned.1.call-start = ((), (), s32[]{:S(2)}) async-start(), calls=%async_computation.5 | async-start | bytes 8519680 | tf_op jit(solution)/shard_map/all_gather | solution.py:58
  89.6 61.3 %copy-start.7 = (f32[2,128,1,256]{1,0,3,2:T(2,128)S(1)}, f32[2,128,1,256]{1,0,3,2:T(2,128)}, u32[]{:S(2)}) copy-start(f32[2,128,1,256]{1,0,3,2:T(2,128)} %copy-done.6) | copy-start | bytes 786436
  90.9 60.2 %copy-start.5 = (bf16[2048,128]{1,0:T(8,128)(2,1)S(1)}, bf16[2048,128]{1,0:T(8,128)(2,1)}, u32[]{:S(2)}) copy-start(bf16[2048,128]{1,0:T(8,128)(2,1)} %param.22) | copy-start | bytes 1572868
  91.0 81.3 %all-to-all-start.1 = ((bf16[64,32,384]{2,1,0:T(8,128)(2,1)}), bf16[64,32,384]{2,1,0:T(8,128)(2,1)}, u32[]{:S(2)}, u32[]{:S(2)}) async-start(bf16[64,32,384]{2,1,0:T(8,128)(2,1)} %stack.2), calls=%async_computation.1 | async-start | bytes 3145728 | tf_op jit(solution)/shard_map/all_to_all | solution.py:67
  160.5 11.8 %copy-start.10 = (f32[256,1]{0,1:T(1,128)S(1)}, f32[256,1]{0,1:T(1,128)}, u32[]{:S(2)}) copy-start(f32[256,1]{0,1:T(1,128)} %param.25) | copy-start | bytes 3076
  172.9 113.7 %all-to-all-start.2 = ((f32[64,256,1]{1,2,0:T(1,128)}), f32[64,256,1]{1,2,0:T(1,128)S(1)}, u32[]{:S(2)}, u32[]{:S(2)}) async-start(f32[64,256,1]{1,2,0:T(1,128)} %broadcast_in_dim.33), calls=%async_computation.2 | async-start | bytes 131072 | tf_op jit(solution)/shard_map/all_to_all | solution.py:25
Sparse Core Ops, SparseCore 0:
  42.1 38.8 all-gather.10
  88.0 72.4 all-gather.6
  163.5 104.4 all-gather.8
